TPU v7x, 32 devices: a whole 2x2x4 slice. The times are simulated.
32 devices in a mesh: rep: 2 (over x), fs: 4 (over z), tp: 4 (over y, core).
Axes of the slice: x: 2, y: 2, z: 4, core: 2. Of those that a mesh axis runs over, the one named last changes fastest.
Arguments:
- tokens: bfloat16 [4096, 2048], P(('rep', 'fs', 'tp')), may hold values from -6 to 6
- mix_gain: bfloat16 [2048], replicated, may hold values from 0.099609375 to 1.8984375
- gate_proj: bfloat16 [2048, 512], P('fs', 'tp'), may hold values from -0.125 to 0.125
- value_proj: bfloat16 [2048, 512], P('fs', 'tp'), may hold values from -1 to 1
- layer_gain: bfloat16 [512], replicated, may hold values from 0.099609375 to 1.8984375
- layer_shift: bfloat16 [512], replicated, may hold values from -3 to 3
- mix_kernel: bfloat16 [4, 128, 128], replicated, may hold values from -0.5 to 0.5
- mix_offset: bfloat16 [4, 128], replicated, may hold values from -4 to 4
- out_proj: bfloat16 [2048, 512], P('fs', 'tp'), may hold values from -0.25 to 0.25
- ffn_gain: bfloat16 [2048], replicated, may hold values from 0.099609375 to 1.8984375
- ffn_gate: bfloat16 [2048, 5632], P('fs', 'tp'), may hold values from -0.125 to 0.125
- ffn_up: bfloat16 [2048, 5632], P('fs', 'tp'), may hold values from -0.125 to 0.125
- ffn_down: bfloat16 [2048, 5632], P('fs', 'tp'), may hold values from -0.078125 to 0.078125
Outputs:
- layer_out: bfloat16 [4096, 2048], P(('rep', 'fs', 'tp'))
All inputs are finite; a program needn't handle non-finite values.
Results may differ from a plain program's by a relative error of at most 0.015.
Values may be sent and summed in bfloat16 or wider, within the bound.
A program may use at most 64 MiB of HBM per device.

v0:
```python
import jax
import jax.numpy as jnp
from jax import lax
from jax.sharding import PartitionSpec as P

epsilon = 1e-06


def rms_norm(rows, gain):
    floats = rows.astype(jnp.float32)
    scale = lax.rsqrt(jnp.mean(floats * floats, axis=-1, keepdims=True) + epsilon)
    return (floats * scale * gain.astype(jnp.float32)).astype(jnp.bfloat16)


def contract_last(left, right):
    return lax.dot_general(
        left, right, (((1,), (1,)), ((), ())), preferred_element_type=jnp.float32
    )


def per_device(
    tokens,
    mix_gain,
    gate_proj,
    value_proj,
    layer_gain,
    layer_shift,
    mix_kernel,
    mix_offset,
    out_proj,
    ffn_gain,
    ffn_gate,
    ffn_up,
    ffn_down,
):
    normed = rms_norm(tokens, mix_gain)
    gate_rows, value_rows, out_rows = (
        lax.all_gather(gate_proj, "fs", axis=0, tiled=True),
        lax.all_gather(value_proj, "fs", axis=0, tiled=True),
        lax.all_gather(out_proj, "fs", axis=0, tiled=True),
    )
    mix_width = layer_gain.shape[0]
    groups = mix_kernel.shape[0]
    span_len = mix_kernel.shape[1]
    causal = jnp.tril(jnp.ones((span_len, span_len), dtype=bool))
    masked = jnp.where(causal[None], mix_kernel, jnp.zeros_like(mix_kernel))
    local_width = gate_rows.shape[1]
    first_col = lax.axis_index("tp") * local_width
    joined = jnp.concatenate([gate_rows, value_rows], axis=1)
    preact = jnp.dot(
        lax.all_gather(normed, "tp", axis=0, tiled=True), joined, preferred_element_type=jnp.float32
    )
    gate_u = jax.nn.gelu(preact[:, :local_width])
    activated = jax.nn.gelu(preact[:, local_width:])
    row_sum, squares = lax.psum(
        (jnp.sum(activated, axis=-1), jnp.sum(activated * activated, axis=-1)), "tp"
    )
    center = (row_sum / mix_width)[:, None]
    spread = (squares / mix_width)[:, None] - center * center
    gain_part = lax.dynamic_slice_in_dim(layer_gain, first_col, local_width).astype(jnp.float32)
    shift_part = lax.dynamic_slice_in_dim(layer_shift, first_col, local_width).astype(jnp.float32)
    values = ((activated - center) * lax.rsqrt(spread + epsilon) * gain_part + shift_part).astype(
        jnp.bfloat16
    )
    group_id = first_col // (mix_width // groups)
    kernel = lax.dynamic_index_in_dim(masked, group_id, 0, keepdims=False)
    offset = lax.dynamic_index_in_dim(mix_offset, group_id, 0, keepdims=False).astype(jnp.float32)
    mixing = jnp.einsum(
        "ts,nsc->ntc",
        kernel,
        values.reshape(-1, span_len, local_width),
        preferred_element_type=jnp.float32,
    )
    mixing = mixing + offset[None, :, None]
    gated_rows = (gate_u * mixing.reshape(gate_u.shape)).astype(jnp.bfloat16)
    mixer_out = lax.psum_scatter(
        contract_last(gated_rows, out_rows).astype(jnp.bfloat16),
        "tp",
        scatter_dimension=0,
        tiled=True,
    ).astype(jnp.float32)
    middle = (tokens.astype(jnp.float32) + mixer_out).astype(jnp.bfloat16)
    normed2 = rms_norm(middle, ffn_gain)
    gathered = lax.all_gather(normed2, "tp", axis=0, tiled=True)
    gate_pre = jnp.dot(
        gathered,
        lax.all_gather(ffn_gate, "fs", axis=0, tiled=True),
        preferred_element_type=jnp.float32,
    )
    up_pre = jnp.dot(
        gathered,
        lax.all_gather(ffn_up, "fs", axis=0, tiled=True),
        preferred_element_type=jnp.float32,
    )
    hidden = (jax.nn.silu(gate_pre) * up_pre).astype(jnp.bfloat16)
    partial_value = contract_last(hidden, lax.all_gather(ffn_down, "fs", axis=0, tiled=True))
    summed = lax.psum_scatter(
        partial_value.astype(jnp.bfloat16), "tp", scatter_dimension=0, tiled=True
    ).astype(jnp.float32)
    return (middle.astype(jnp.float32) + summed).astype(jnp.bfloat16)


def solution(mesh):
    placed = (
        P(("rep", "fs", "tp"), None),
        P(),
        P("fs", "tp"),
        P("fs", "tp"),
        P(),
        P(),
        P(),
        P(),
        P("fs", "tp"),
        P(),
        P("fs", "tp"),
        P("fs", "tp"),
        P("fs", "tp"),
    )
    return jax.shard_map(
        per_device,
        mesh=mesh,
        in_specs=placed,
        out_specs=P(("rep", "fs", "tp"), None),
        check_vma=False,
    )
```

profile of v0, /device:TPU:1, one launch (start us, length us, event | category | flops | bytes accessed | tf_op | source)
XLA Modules:
  0.0 471.9 jit_solution(3375747574779029369)
XLA Ops:
  7.4 0.7 convert_element_type.64
  8.1 1.2 fusion.1
  9.3 2.0 fusion.3
  11.4 0.0 reduce-scatter.3.cloned.1.call-start
  11.5 0.7 bitcast_convert_fusion
  12.2 0.8 dynamic-slice_convert_fusion
  12.9 15.5 %all_gather.25 = bf16[2048,128]{1,0:T(8,128)(2,1)S(1)} all-gather(bf16[512,128]{1,0:T(8,128)(2,1)} %param.15), channel_id=1, replica_groups=mesh['rep'=2,'fs'=4,'tp'=4] {'fs'}, dimensions={0}, use_global_device_ids=true | all-gather | bytes 655360 | tf_op jit(solution)/shard_map/all_gather | solution.py:38
  28.5 11.9 %all_gather.26 = bf16[2048,128]{1,0:T(8,128)(2,1)S(1)} all-gather(bf16[512,128]{1,0:T(8,128)(2,1)S(1)} %copy-done.2), channel_id=1, replica_groups=mesh['rep'=2,'fs'=4,'tp'=4] {'fs'}, dimensions={0}, use_global_device_ids=true | all-gather | bytes 655360 | tf_op jit(solution)/shard_map/all_gather | solution.py:39
  40.3 13.6 %all_gather.27 = bf16[2048,128]{1,0:T(8,128)(2,1)S(1)} all-gather(bf16[512,128]{1,0:T(8,128)(2,1)S(1)} %copy-done.3), channel_id=1, replica_groups=mesh['rep'=2,'fs'=4,'tp'=4] {'fs'}, dimensions={0}, use_global_device_ids=true | all-gather | bytes 655360 | tf_op jit(solution)/shard_map/all_gather | solution.py:40
  53.9 2.3 fusion.9
  56.2 0.2 fusion.37
  56.5 14.0 %all-reduce = (f32[512]{0:T(512)S(1)}, f32[512]{0:T(512)S(1)}) all-reduce(f32[512]{0:T(512)S(1)} %get-tuple-element.6, f32[512]{0:T(512)S(1)} %get-tuple-element.5), channel_id=1, replica_groups=mesh['rep'=2,'fs'=4,'tp'=4] {'tp'}, use_global_device_ids=true, to_apply=%region_4.5 | all-reduce | flops 1024 | bytes 8192 | tf_op jit(solution)/shard_map/psum | solution.py:55
  70.4 0.2 add_convert_fusion
  70.7 0.9 convolution_add_fusion
  71.6 0.1 fusion.21
  71.7 2.1 convolution_convert_fusion
  73.8 0.0 all-gather.10.cloned.1.call-start
  73.9 0.5 all-gather.10.cloned.1.call-update
  74.5 31.2 %reduce-scatter.3.cloned.1.call-done = bf16[128,2048]{1,0:T(8,128)(2,1)} async-done(((bf16[512,2048]{1,0:T(8,128)(2,1)}), bf16[128,2048]{1,0:T(8,128)(2,1)}) %reduce-scatter.3.cloned.1.call-update) | async-done | bytes 524304 | tf_op jit(solution)/shard_map/reduce_scatter | solution.py:76
  105.7 1.3 fusion.5
  107.0 2.0 fusion.7
  109.1 0.0 all-gather.12.cloned.1.call-start
  109.1 0.5 all-gather.12.cloned.1.call-update
  109.7 0.7 all-gather.14.cloned.1.call-update
  110.5 72.8 %all-gather.10.cloned.1.call-done = bf16[2048,1408]{1,0:T(8,128)(2,1)} async-done(((bf16[512,1408]{1,0:T(8,128)(2,1)}), bf16[2048,1408]{1,0:T(8,128)(2,1)}) %all-gather.10.cloned.1.call-update) | async-done | bytes 5767184 | tf_op jit(solution)/shard_map/all_gather | solution.py:87
  183.3 22.5 %all-gather.8.cloned.1.call-done = bf16[512,2048]{1,0:T(8,128)(2,1)} async-done(((bf16[128,2048]{1,0:T(8,128)(2,1)}), bf16[512,2048]{1,0:T(8,128)(2,1)}) %all-gather.8.cloned.1.call-update) | async-done | bytes 2097168 | tf_op jit(solution)/shard_map/all_gather | solution.py:84
  205.7 8.4 %fusion.38 = f32[512,1408]{1,0:T(8,128)} fusion(bf16[512,2048]{1,0:T(8,128)(2,1)} %all-gather.8.cloned.1.call-done, bf16[2048,1408]{1,0:T(8,128)(2,1)} %all-gather.10.cloned.1.call-done), kind=kOutput, calls=%fused_computation.60 | convolution fusion | flops 2952790016 | bytes 10747904 | tf_op jit(solution)/shard_map/dot_general | solution.py:85
  214.1 99.3 %all-gather.12.cloned.1.call-done = bf16[2048,1408]{1,0:T(8,128)(2,1)} async-done(((bf16[512,1408]{1,0:T(8,128)(2,1)}), bf16[2048,1408]{1,0:T(8,128)(2,1)}) %all-gather.12.cloned.1.call-update) | async-done | bytes 5767184 | tf_op jit(solution)/shard_map/all_gather | solution.py:92
  313.5 106.4 %all-gather.14.cloned.1.call-done = bf16[2048,1408]{1,0:T(8,128)(2,1)} async-done(((bf16[512,1408]{1,0:T(8,128)(2,1)}), bf16[2048,1408]{1,0:T(8,128)(2,1)}) %all-gather.14.cloned.1.call-update) | async-done | bytes 5767184 | tf_op jit(solution)/shard_map/all_gather | solution.py:96
  419.9 13.2 %convolution_convert_fusion.1 = bf16[512,2048]{1,0:T(8,128)(2,1)} fusion(bf16[2048,1408]{1,0:T(8,128)(2,1)} %all-gather.14.cloned.1.call-done, bf16[512,2048]{1,0:T(8,128)(2,1)S(1)} %copy-done.5, bf16[2048,1408]{1,0:T(8,128)(2,1)} %all-gather.12.cloned.1.call-done, f32[512,1408]{1,0:T(8,128)} %fusion.38), kind=kOutput, calls=%fused_computation.3 | convolution fusion | flops 5910953984 | bytes 18612224 | tf_op jit(solution)/shard_map/dot_general | solution.py:16
  433.1 29.3 %reduce-scatter.5.cloned.1.call-done = bf16[128,2048]{1,0:T(8,128)(2,1)} async-done(((bf16[512,2048]{1,0:T(8,128)(2,1)}), bf16[128,2048]{1,0:T(8,128)(2,1)}) %reduce-scatter.5.cloned.1.call-update) | async-done | bytes 524304 | tf_op jit(solution)/shard_map/reduce_scatter | solution.py:97
  462.5 2.1 fusion.8
  (26 shorter events, 0.3 us)
Async XLA Ops:
  7.4 21.1 %copy-start.2 = (bf16[512,128]{1,0:T(8,128)(2,1)S(1)}, bf16[512,128]{1,0:T(8,128)(2,1)}, u32[]{:S(2)}) copy-start(bf16[512,128]{1,0:T(8,128)(2,1)} %param.16) | copy-start | bytes 393220
  7.4 33.0 %copy-start.3 = (bf16[512,128]{1,0:T(8,128)(2,1)S(1)}, bf16[512,128]{1,0:T(8,128)(2,1)}, u32[]{:S(2)}) copy-start(bf16[512,128]{1,0:T(8,128)(2,1)} %param.21) | copy-start | bytes 393220
  7.4 46.5 %all-gather.6.cloned.1.call-start = ((), (), s32[]{:S(2)}) async-start(), calls=%async_computation.2 | async-start | bytes 2621440 | tf_op jit(solution)/shard_map/all_gather | solution.py:51
  11.4 94.3 %reduce-scatter.3.cloned.1.call-start = ((), (), s32[]{:S(2)}) async-start(), calls=%async_computation.3 | async-start | bytes 2621440 | tf_op jit(solution)/shard_map/reduce_scatter | solution.py:76
  71.7 2.7 copy-start.4
  71.7 34.0 %copy-start = (bf16[128,2048]{1,0:T(8,128)(2,1)S(1)}, bf16[128,2048]{1,0:T(8,128)(2,1)}, u32[]{:S(2)}) copy-start(bf16[128,2048]{1,0:T(8,128)(2,1)} %param.13) | copy-start | bytes 1572868
  73.8 109.5 %all-gather.10.cloned.1.call-start = ((), (), s32[]{:S(2)}) async-start(), calls=%async_computation.5 | async-start | bytes 7208960 | tf_op jit(solution)/shard_map/all_gather | solution.py:87
  74.4 131.3 %all-gather.8.cloned.1.call-start = ((), (), s32[]{:S(2)}) async-start(), calls=%async_computation.4 | async-start | bytes 2621440 | tf_op jit(solution)/shard_map/all_gather | solution.py:84
  109.1 204.4 %all-gather.12.cloned.1.call-start = ((), (), s32[]{:S(2)}) async-start(), calls=%async_computation.6 | async-start | bytes 7208960 | tf_op jit(solution)/shard_map/all_gather | solution.py:92
  109.7 310.2 %all-gather.14.cloned.1.call-start = ((), (), s32[]{:S(2)}) async-start(), calls=%async_computation.7 | async-start | bytes 7208960 | tf_op jit(solution)/shard_map/all_gather | solution.py:96
  110.4 352.1 %reduce-scatter.5.cloned.1.call-start = ((), (), s32[]{:S(2)}) async-start(), calls=%async_computation.8 | async-start | bytes 2621440 | tf_op jit(solution)/shard_map/reduce_scatter | solution.py:97
  205.7 214.1 %copy-start.5 = (bf16[512,2048]{1,0:T(8,128)(2,1)S(1)}, bf16[512,2048]{1,0:T(8,128)(2,1)}, u32[]{:S(2)}) copy-start(bf16[512,2048]{1,0:T(8,128)(2,1)} %all-gather.8.cloned.1.call-done) | copy-start | bytes 6291460
  214.1 248.4 %copy-start.1 = (bf16[128,2048]{1,0:T(8,128)(2,1)S(1)}, bf16[128,2048]{1,0:T(8,128)(2,1)}, u32[]{:S(2)}) copy-start(bf16[128,2048]{1,0:T(8,128)(2,1)} %reduce-scatter.3.cloned.1.call-done) | copy-start | bytes 1572868
Sparse Core Ops, SparseCore 0:
  11.5 25.0 all-gather.5
  73.9 31.7 reduce-scatter.2
  433.2 29.1 reduce-scatter.4
Sparse Core Ops, SparseCore 1:
  75.9 107.4 all-gather.9
  184.7 21.0 all-gather.7
  207.2 106.2 all-gather.11
  315.1 104.8 all-gather.13
where the time goes:
time: 473 us; the launch traced here: 472 us
  waiting for transfers between devices  363 us (77%)
  blocking collectives  54.9 us (12%)
  matrix products  26.9 us (6%)
  between operations  14.9 us (3%)
  other arithmetic  11.5 us (2%)
    all_gather x1, waiting for transfers between devices, per_device(): lax.all_gather(ffn_down, 'fs', axis=0, tiled=True)  106 us
    all_gather x1, waiting for transfers between devices, per_device(): lax.all_gather(ffn_up, 'fs', axis=0, tiled=True)  99.3 us
    all_gather x1, waiting for transfers between devices, per_device(): lax.all_gather(ffn_gate, 'fs', axis=0, tiled=True)  72.8 us
    reduce_scatter x1, waiting for transfers between devices, per_device(): lax.psum_scatter(contract_last(gated_rows, out_rows).astype(jnp.bfloat16)...  31.2 us
    reduce_scatter x1, waiting for transfers between devices, per_device(): lax.psum_scatter(partial_value.astype(jnp.bfloat16), 'tp', scatter_dimens...  29.3 us
    all_gather x1, waiting for transfers between devices, per_device(): gathered = lax.all_gather(normed2, 'tp', axis=0, tiled=True)  22.5 us
    all_gather x1, blocking collectives, per_device(): lax.all_gather(gate_proj, 'fs', axis=0, tiled=True)  15.5 us
    dot_general x2, matrix products, contract_last(): lax.dot_general(left, right, (((1,), (1,)), ((), ())), preferred_element_...  15.3 us
  transfers between devices with their start and end apart: 7, of which 6 were waited for; matrix products, arithmetic and copies ran while one was open for 3% of the time, Pallas kernels for 0%

commit v1 on v0

v1 whole, which is shorter than its diff:
```python
import functools

import jax
import jax.numpy as jnp
from jax import lax
from jax.experimental import pallas as pl
from jax.experimental.pallas import tpu as pltpu
from jax.sharding import PartitionSpec as P

epsilon = 1e-06
MESH = pl.DeviceIdType.MESH
F32 = jnp.float32
BF16 = jnp.bfloat16


def rms_norm(floats, gain):
    scale = lax.rsqrt(jnp.mean(floats * floats, axis=-1, keepdims=True) + epsilon)
    return (floats * scale * gain).astype(BF16)


def gelu(x):
    inner = 0.7978845608028654 * (x + 0.044715 * (x * x * x))
    return 0.5 * x * (1.0 + jnp.tanh(inner))


def contract_last(left, right):
    return lax.dot_general(left, right, (((1,), (1,)), ((), ())), preferred_element_type=F32)


def kernel(
    sizes,
    tok_ref,
    mg_ref,
    lg_ref,
    ls_ref,
    mk_ref,
    mo_ref,
    fg_ref,
    m_ref,
    g_ref,
    d_ref,
    out_ref,
    mbuf,
    gbuf,
    dbuf,
    nall,
    gate_u,
    act,
    stats,
    obuf,
    orecv,
    mid,
    xall,
    hbuf,
    pbuf,
    prow,
    ring_s,
    ring_r,
    n_s,
    n_r,
    st_s,
    st_r,
    o_s,
    o_r,
    x_s,
    x_r,
    p_s,
    p_r,
):
    n_rep, n_fs, n_tp, width, lw, lwp, group_ch, half = sizes
    tok, model = tok_ref.shape
    depth = m_ref.shape[0]
    part = depth // 2
    rep, fs, tp = lax.axis_index("rep"), lax.axis_index("fs"), lax.axis_index("tp")
    n_g = n_rep * n_tp
    g_id = rep * n_tp + tp
    right = lax.rem(fs + 1, n_fs)
    left = lax.rem(fs + n_fs - 1, n_fs)

    def group_peer(d):
        other = lax.rem(g_id + d, n_g)
        return other, {"rep": other // n_tp, "tp": lax.rem(other, n_tp)}

    def tp_peer(d):
        other = lax.rem(tp + d, n_tp)
        return other, {"tp": other}

    barrier = pltpu.get_barrier_semaphore()
    for side in (left, right):
        pl.semaphore_signal(barrier, inc=1, device_id={"fs": side}, device_id_type=MESH)
    for d in range(1, n_g):
        pl.semaphore_signal(barrier, inc=1, device_id=group_peer(d)[1], device_id_type=MESH)
    pl.semaphore_wait(barrier, n_g + 1)

    held = ((m_ref, mbuf), (g_ref, gbuf), (d_ref, dbuf))

    def block(p, s):
        return held[p][0] if s == 0 else held[p][1].at[s - 1]

    def ring(p, h, s):
        rows = pl.ds(h * part, part)
        return pltpu.make_async_remote_copy(
            src_ref=block(p, s - 1).at[rows],
            dst_ref=block(p, s).at[rows],
            send_sem=ring_s.at[p, h, s - 1],
            recv_sem=ring_r.at[p, h, s - 1],
            device_id={"fs": right},
            device_id_type=MESH,
        )

    def columns(s, size=None):
        size = depth if size is None else size
        owner = lax.rem(fs - s + n_fs, n_fs)
        return pl.multiple_of(owner * depth, 128)

    ring(0, 0, 1).start()
    ring(0, 1, 1).start()

    nmine = pl.ds(pl.multiple_of(tp * tok, tok), tok)
    nall[nmine, :] = rms_norm(tok_ref[...].astype(F32), mg_ref[...].astype(F32))

    def ncopy(d):
        return pltpu.make_async_remote_copy(
            src_ref=nall.at[nmine],
            dst_ref=nall.at[nmine],
            send_sem=n_s.at[d - 1],
            recv_sem=n_r.at[d - 1],
            device_id=tp_peer(d)[1],
            device_id_type=MESH,
        )

    for d in range(1, n_tp):
        ncopy(d).start()
    for s in range(2, n_fs):
        for h in range(2):
            ring(0, h, s - 1).wait_recv()
            ring(0, h, s).start()
    ring(1, 0, 1).start()
    ring(1, 1, 1).start()
    for h in range(2):
        ring(0, h, n_fs - 1).wait_recv()
    for d in range(1, n_tp):
        ncopy(d).wait_recv()

    rows_tp = n_tp * tok

    def project(i, carry):
        rows = pl.ds(pl.multiple_of(i * tok, tok), tok)
        pre = jnp.zeros((tok, 2 * lwp), F32)
        for s in range(n_fs):
            pre = pre + jnp.dot(
                nall[rows, pl.ds(columns(s), depth)],
                block(0, s)[:, : 2 * lwp],
                preferred_element_type=F32,
            )
        gate_u[rows, :] = gelu(pre[:, :lwp])
        a = gelu(pre[:, lwp:])
        act[rows, :] = a
        flipped = a.T
        one = jnp.sum(flipped, axis=0, keepdims=True)
        two = jnp.sum(flipped * flipped, axis=0, keepdims=True)
        which = lax.broadcasted_iota(jnp.int32, (8, tok), 0)
        stats[0, i] = jnp.where(which == 0, one, two)
        return carry

    lax.fori_loop(0, n_tp, project, 0)

    def stcopy(d):
        return pltpu.make_async_remote_copy(
            src_ref=stats.at[0],
            dst_ref=stats.at[d],
            send_sem=st_s.at[d - 1],
            recv_sem=st_r.at[d - 1],
            device_id=tp_peer(d)[1],
            device_id_type=MESH,
        )

    for d in range(1, n_tp):
        stcopy(d).start()
    for d in range(1, n_tp):
        stcopy(d).wait_recv()

    group = (tp * lw) // group_ch
    span = mk_ref.shape[1]
    at_t = lax.broadcasted_iota(jnp.int32, (span, span), 0)
    at_s = lax.broadcasted_iota(jnp.int32, (span, span), 1)
    mix_k = jnp.where(at_s <= at_t, mk_ref[group].astype(F32), 0.0).astype(BF16)
    gain_part, shift_part, offset = lg_ref[tp], ls_ref[tp], mo_ref[group]

    def mix(i, carry):
        rows = pl.ds(pl.multiple_of(i * tok, tok), tok)
        total = stats[0, i]
        for d in range(1, n_tp):
            total = total + stats[d, i]
        flipped = jnp.concatenate([total] * 16, axis=0).T
        center = flipped[:, 0:1] / width
        spread = flipped[:, 1:2] / width - center * center
        values = (
            (act[rows, :] - center) * lax.rsqrt(spread + epsilon) * gain_part + shift_part
        ).astype(BF16)
        gates = gate_u[rows, :]
        for b in range(tok // span):
            cut = slice(b * span, (b + 1) * span)
            mixing = jnp.dot(mix_k, values[cut], preferred_element_type=F32) + offset
            gated = (gates[cut] * mixing).astype(BF16)
            to = pl.ds(pl.multiple_of(i * tok + b * span, span), span)
            for s in range(n_fs):
                obuf[to, pl.ds(columns(s), depth)] = contract_last(
                    gated, block(0, s)[:, 2 * lwp :]
                ).astype(BF16)
        return carry

    lax.fori_loop(0, n_tp, mix, 0)

    def ocopy(d):
        other, where = tp_peer(d)
        return pltpu.make_async_remote_copy(
            src_ref=obuf.at[pl.ds(pl.multiple_of(other * tok, tok), tok)],
            dst_ref=orecv.at[d - 1],
            send_sem=o_s.at[d - 1],
            recv_sem=o_r.at[d - 1],
            device_id=where,
            device_id_type=MESH,
        )

    for d in range(1, n_tp):
        ocopy(d).start()

    steps = [(h, s) for s in range(2, n_fs) for h in range(2)]
    cut = len(steps) // 2
    for h, s in steps[:cut]:
        ring(1, h, s - 1).wait_recv()
        ring(1, h, s).start()

    for d in range(1, n_tp):
        ocopy(d).wait_recv()
    mixer_out = obuf[nmine, :].astype(F32)
    for d in range(1, n_tp):
        mixer_out = mixer_out + orecv[d - 1].astype(F32)
    middle = (tok_ref[...].astype(F32) + mixer_out).astype(BF16)
    mid[...] = middle
    xmine = pl.ds(pl.multiple_of(g_id * tok, tok), tok)
    xall[xmine, :] = rms_norm(middle.astype(F32), fg_ref[...].astype(F32))

    def xcopy(d):
        return pltpu.make_async_remote_copy(
            src_ref=xall.at[xmine],
            dst_ref=xall.at[xmine],
            send_sem=x_s.at[d - 1],
            recv_sem=x_r.at[d - 1],
            device_id=group_peer(d)[1],
            device_id_type=MESH,
        )

    for d in range(1, n_g):
        xcopy(d).start()
    for h, s in steps[cut:]:
        ring(1, h, s - 1).wait_recv()
        ring(1, h, s).start()
    ring(2, 0, 1).start()
    ring(2, 1, 1).start()
    for d in range(1, n_g):
        xcopy(d).wait_recv()
    for h in range(2):
        ring(1, h, n_fs - 1).wait_recv()

    gu = g_ref.shape[1]
    hid = d_ref.shape[1]
    chunk = 2 * tok

    def feed(i, carry):
        rows = pl.ds(pl.multiple_of(i * chunk, chunk), chunk)
        pre = jnp.zeros((chunk, gu), F32)
        for s in range(n_fs):
            pre = pre + jnp.dot(
                xall[rows, pl.ds(columns(s), depth)],
                block(1, s)[...],
                preferred_element_type=F32,
            )
        gate = pre[:, :hid]
        if gu == 2 * hid:
            up = pre[:, hid:]
        else:
            up = pltpu.roll(pre, gu - half, 1)[:, :hid]
        hidden = gate * lax.logistic(gate) * up
        if gu != 2 * hid:
            lane = lax.broadcasted_iota(jnp.int32, hidden.shape, 1)
            hidden = jnp.where(lane < half, hidden, 0.0)
        hbuf[rows, :] = hidden.astype(BF16)
        return carry

    lax.fori_loop(0, n_g // 2, feed, 0)

    def pcols(s, h):
        return pl.ds(pl.multiple_of(columns(s) + h * part, part), part)

    def down(s, h):
        weights = block(2, s)[h * part : (h + 1) * part, :]

        def one(i, carry):
            rows = pl.ds(pl.multiple_of(i * chunk, chunk), chunk)
            pbuf[s, h, rows, :] = contract_last(hbuf[rows, :], weights).astype(BF16)
            return carry

        lax.fori_loop(0, n_g // 2, one, 0)

    def pcopy(s, h, d):
        other, where = group_peer(d)
        return pltpu.make_async_remote_copy(
            src_ref=pbuf.at[s, h, pl.ds(pl.multiple_of(other * tok, tok), tok)],
            dst_ref=prow.at[s, h, d - 1],
            send_sem=p_s.at[s, h, d - 1],
            recv_sem=p_r.at[s, h, d - 1],
            device_id=where,
            device_id_type=MESH,
        )

    for s in range(n_fs):
        for h in range(2):
            if s > 0:
                ring(2, h, s).wait_recv()
                if s < n_fs - 1:
                    ring(2, h, s + 1).start()
            down(s, h)
            for d in range(1, n_g):
                pcopy(s, h, d).start()
    for s in range(n_fs):
        owner = lax.rem(fs - s + n_fs, n_fs)
        for h in range(2):
            for d in range(1, n_g):
                pcopy(s, h, d).wait_recv()
            total = pbuf[s, h, xmine, :].astype(F32)
            for d in range(1, n_g):
                total = total + prow[s, h, d - 1].astype(F32)
            for o in range(n_fs):

                @pl.when(owner == o)
                def _():
                    cols = slice(o * depth + h * part, o * depth + (h + 1) * part)
                    out_ref[:, cols] = (mid[:, cols].astype(F32) + total).astype(BF16)

    for p in range(3):
        for h in range(2):
            for s in range(1, n_fs):
                ring(p, h, s).wait_send()
    for d in range(1, n_tp):
        ncopy(d).wait_send()
        stcopy(d).wait_send()
        ocopy(d).wait_send()
    for d in range(1, n_g):
        xcopy(d).wait_send()
        for s in range(n_fs):
            for h in range(2):
                pcopy(s, h, d).wait_send()


def round_up(n, m):
    return (n + m - 1) // m * m


def pad_last(x, size):
    return jnp.pad(x, [(0, 0)] * (x.ndim - 1) + [(0, size - x.shape[-1])])


def per_device(
    mesh_sizes,
    tokens,
    mix_gain,
    gate_proj,
    value_proj,
    layer_gain,
    layer_shift,
    mix_kernel,
    mix_offset,
    out_proj,
    ffn_gain,
    ffn_gate,
    ffn_up,
    ffn_down,
):
    n_rep, n_fs, n_tp = mesh_sizes
    tok, model = tokens.shape
    depth, lw = gate_proj.shape
    lwp = round_up(lw, 128)
    width = layer_gain.shape[0]
    groups = mix_kernel.shape[0]
    half = ffn_gate.shape[1] // n_rep
    hid = round_up(half, 128)
    first = lax.axis_index("rep") * half
    gate_half, up_half, down_half = (
        lax.dynamic_slice_in_dim(x, first, half, axis=1) for x in (ffn_gate, ffn_up, ffn_down)
    )
    if (2 * half) % 128 == 0 and half % 128 != 0 and 2 * half >= hid and (2 * half) % 256 == 128:
        gu = jnp.concatenate([gate_half, up_half], axis=1)
    else:
        gu = jnp.concatenate([pad_last(gate_half, hid), pad_last(up_half, hid)], axis=1)
    down = pad_last(down_half, hid)
    mixw = jnp.concatenate([pad_last(x, lwp) for x in (gate_proj, value_proj, out_proj)], axis=1)
    lgain = pad_last(layer_gain.astype(F32).reshape(n_tp, 1, lw), lwp)
    lshift = pad_last(layer_shift.astype(F32).reshape(n_tp, 1, lw), lwp)
    offset = mix_offset.astype(F32)[:, :, None]
    n_g = n_rep * n_tp
    guw = gu.shape[1]
    part = depth // 2
    sizes = (n_rep, n_fs, n_tp, width, lw, lwp, width // groups, half)
    vmem = pl.BlockSpec(memory_space=pltpu.VMEM)
    dma = pltpu.SemaphoreType.DMA
    return pl.pallas_call(
        functools.partial(kernel, sizes),
        out_shape=jax.ShapeDtypeStruct((tok, model), BF16),
        in_specs=[vmem] * 10,
        out_specs=vmem,
        scratch_shapes=[
            pltpu.VMEM((n_fs - 1, depth, 3 * lwp), BF16),
            pltpu.VMEM((n_fs - 1, depth, guw), BF16),
            pltpu.VMEM((n_fs - 1, depth, hid), BF16),
            pltpu.VMEM((n_tp * tok, model), BF16),
            pltpu.VMEM((n_tp * tok, lwp), F32),
            pltpu.VMEM((n_tp * tok, lwp), F32),
            pltpu.VMEM((n_tp, n_tp, 8, tok), F32),
            pltpu.VMEM((n_tp * tok, model), BF16),
            pltpu.VMEM((n_tp - 1, tok, model), BF16),
            pltpu.VMEM((tok, model), BF16),
            pltpu.VMEM((n_g * tok, model), BF16),
            pltpu.VMEM((n_g * tok, hid), BF16),
            pltpu.VMEM((n_fs, 2, n_g * tok, part), BF16),
            pltpu.VMEM((n_fs, 2, n_g - 1, tok, part), BF16),
            dma((3, 2, n_fs - 1)),
            dma((3, 2, n_fs - 1)),
            dma((n_tp - 1,)),
            dma((n_tp - 1,)),
            dma((n_tp - 1,)),
            dma((n_tp - 1,)),
            dma((n_tp - 1,)),
            dma((n_tp - 1,)),
            dma((n_g - 1,)),
            dma((n_g - 1,)),
            dma((n_fs, 2, n_g - 1)),
            dma((n_fs, 2, n_g - 1)),
        ],
        compiler_params=pltpu.CompilerParams(
            collective_id=0, has_side_effects=True, vmem_limit_bytes=67043328
        ),
    )(
        tokens,
        mix_gain.reshape(1, -1),
        lgain,
        lshift,
        mix_kernel,
        offset,
        ffn_gain.reshape(1, -1),
        mixw,
        gu,
        down,
    )


def solution(mesh):
    placed = (
        P(("rep", "fs", "tp"), None),
        P(),
        P("fs", "tp"),
        P("fs", "tp"),
        P(),
        P(),
        P(),
        P(),
        P("fs", "tp"),
        P(),
        P("fs", "tp"),
        P("fs", "tp"),
        P("fs", "tp"),
    )
    mesh_sizes = tuple(mesh.shape[a] for a in ("rep", "fs", "tp"))
    return jax.shard_map(
        functools.partial(per_device, mesh_sizes),
        mesh=mesh,
        in_specs=placed,
        out_specs=P(("rep", "fs", "tp"), None),
        check_vma=False,
    )
```

time: 473 us -> 200 us (0.42)
  waiting for transfers between devices: 363 us -> 0 us
  Pallas kernels: 0 us -> 189 us
  blocking collectives: 54.9 us -> 0 us
  matrix products: 26.9 us -> 0 us
  between operations: 14.9 us -> 0.07 us
  other arithmetic: 11.5 us -> 3.52 us
  local copies, waits for them, and re-layouts: 0.03 us -> 7.83 us
    all_gather x5 -> x0, waiting for transfers between devices: 301 us -> none  [the longest x1 106 us: per_device(): lax.all_gather(ffn_down, 'fs', axis=0, tiled=True)]
    pallas_call x0 -> x1, Pallas kernels: none -> 189 us  [per_device(): pl.pallas_call(functools.partial(kernel, sizes), out_shape=jax.ShapeDtype...]
    reduce_scatter x2 -> x0, waiting for transfers between devices: 60.6 us -> none  [the longest x1 31.2 us: per_device(): lax.psum_scatter(contract_last(gated_rows, out_rows).astype(jnp.bfloat16)...]
    all_gather x3 -> x0, blocking collectives: 41 us -> none  [the longest x1 15.5 us: per_device(): lax.all_gather(gate_proj, 'fs', axis=0, tiled=True)]
    dot_general x5 -> x0, matrix products: 26.9 us -> none  [the longest x2 15.3 us: contract_last(): lax.dot_general(left, right, (((1,), (1,)), ((), ())), preferred_element_...]
    psum x1 -> x0, blocking collectives: 14 us -> none  [per_device(): lax.psum((jnp.sum(activated, axis=-1), jnp.sum(activated * activated, axi...]
    convert_element_type x9 -> x0, other arithmetic: 8.66 us -> none  [the longest x4 4.81 us: rms_norm(): return (floats * scale * gain.astype(jnp.float32)).astype(jnp.bfloat16)]
  transfers between devices with their start and end apart: 7 -> 0, of which waited for: 6 -> 0; matrix products, arithmetic and copies ran while one was open for 3% -> 0% of each run, Pallas kernels for 0% -> 0%
where the time goes in v1:
time: 200 us
  Pallas kernels  189 us (94%)
  local copies, waits for them, and re-layouts  7.83 us (4%)
  other arithmetic  3.52 us (2%)
    pallas_call x1, Pallas kernels, per_device(): pl.pallas_call(functools.partial(kernel, sizes), out_shape=jax.ShapeDtype...  189 us

profile of v1, /device:TPU:1, one launch (start us, length us, event | category | flops | bytes accessed | tf_op | source)
XLA Modules:
  0.0 200.1 jit_solution(5201737616495659251)
XLA Ops:
  0.0 0.0 copy-start
  0.0 2.3 %constant_dynamic-slice_fusion = (bf16[512,704]{1,0:T(8,128)(2,1)S(1)}, bf16[512,704]{1,0:T(8,128)(2,1)S(1)}) fusion(bf16[512,1408]{1,0:T(8,128)(2,1)} %param.25, s32[]{:T(128)S(6)} %select_n.2, bf16[512,1408]{1,0:T(8,128)(2,1)} %param.24), kind=kLoop, calls=%fused_computation.3 | loop fusion | bytes 2883588 | tf_op jit(solution)/shard_map/dynamic_slice | solution.py:391
  2.3 0.0 copy-done
  2.3 0.5 constant_dynamic-slice_fusion.2
  2.8 1.6 pad_maximum_fusion.g_ref
  4.3 0.0 copy-start.1
  4.3 0.0 copy-start.2
  4.3 0.0 copy-start.3
  4.3 0.0 copy-start.6
  4.3 0.0 copy-start.4
  4.4 0.0 copy-start.5
  4.4 0.0 copy-start.7
  4.4 0.0 copy-start.8
  4.4 1.0 pad.4.d_ref
  5.4 0.0 copy-done.1
  5.4 0.0 copy-done.2
  5.4 0.1 copy-done.3
  5.5 0.8 pad_maximum_fusion.1.m_ref
  6.3 0.0 copy-done.6
  6.3 0.9 copy.14.mo_ref
  7.1 0.0 copy-done.4
  7.1 0.6 reshape.16.mg_ref
  7.8 0.0 copy-done.5
  7.8 0.6 reshape.21.fg_ref
  8.4 0.0 copy-done.7
  8.4 0.6 reshape.22
  9.0 0.0 copy-done.8
  9.0 0.6 reshape.24
  9.5 188.7 %shard_map.127 = bf16[128,2048]{1,0:T(8,128)(2,1)} custom-call(bf16[128,2048]{1,0:T(8,128)(2,1)} %tok_ref.1, bf16[1,2048]{1,0:T(2,128)(2,1)} %reshape.16.mg_ref, f32[4,1,128]{2,1,0:T(1,128)} %bitcast.5, f32[4,1,128]{2,1,0:T(1,128)} %bitcast.6, bf16[4,128,128]{2,1,0:T(8,128)(2,1)} %mk_ref.1, f32[4,128,1]{2,1,0:T(8,128)} %copy.14.mo_ref, ...), custom_call_target="tpu_custom_call" | custom-call | tf_op jit(solution)/shard_map/pallas_call | solution.py:408
  198.3 1.9 copy.16
  (1 shorter events, 0.0 us)
Async XLA Ops:
  0.0 2.3 %copy-start = (bf16[512,1408]{1,0:T(8,128)(2,1)S(1)}, bf16[512,1408]{1,0:T(8,128)(2,1)}, u32[]{:S(2)}) copy-start(bf16[512,1408]{1,0:T(8,128)(2,1)} %param.23) | copy-start | bytes 4325380
  4.3 1.0 copy-start.1
  4.3 1.0 copy-start.2
  4.3 1.1 copy-start.3
  4.3 1.9 copy-start.6
  4.3 2.8 %copy-start.4 = (bf16[2048]{0:T(1024)(128)(2,1)S(1)}, bf16[2048]{0:T(1024)(128)(2,1)}, u32[]{:S(2)}) copy-start(bf16[2048]{0:T(1024)(128)(2,1)} %param.14) | copy-start | bytes 12292
  4.4 3.4 %copy-start.5 = (bf16[2048]{0:T(1024)(128)(2,1)S(1)}, bf16[2048]{0:T(1024)(128)(2,1)}, u32[]{:S(2)}) copy-start(bf16[2048]{0:T(1024)(128)(2,1)} %param.22) | copy-start | bytes 12292
  4.4 4.0 %copy-start.7 = (bf16[512]{0:T(512)(128)(2,1)S(1)}, bf16[512]{0:T(512)(128)(2,1)}, u32[]{:S(2)}) copy-start(bf16[512]{0:T(512)(128)(2,1)} %param.17) | copy-start | bytes 3076
  4.4 4.6 %copy-start.8 = (bf16[512]{0:T(512)(128)(2,1)S(1)}, bf16[512]{0:T(512)(128)(2,1)}, u32[]{:S(2)}) copy-start(bf16[512]{0:T(512)(128)(2,1)} %param.18) | copy-start | bytes 3076

commit v2 on v1

--- a/solution.py
+++ b/solution.py
@@ -56,6 +56,8 @@
     prow,
     ring_s,
     ring_r,
+    e_s,
+    e_r,
     n_s,
     n_r,
     st_s,
@@ -97,8 +99,15 @@
     def block(p, s):
         return held[p][0] if s == 0 else held[p][1].at[s - 1]
 
+    share = depth // n_rep
+    piece = share // 2
+
+    def mixer_rows(h):
+        return pl.ds(pl.multiple_of(rep * share + h * piece, piece), piece)
+
     def ring(p, h, s):
-        rows = pl.ds(h * part, part)
+        size = d_ref.shape[0] // 2 if p == 2 else part
+        rows = mixer_rows(h) if p == 0 else pl.ds(h * size, size)
         return pltpu.make_async_remote_copy(
             src_ref=block(p, s - 1).at[rows],
             dst_ref=block(p, s).at[rows],
@@ -108,8 +117,17 @@
             device_id_type=MESH,
         )
 
-    def columns(s, size=None):
-        size = depth if size is None else size
+    def across(h, s, e):
+        return pltpu.make_async_remote_copy(
+            src_ref=mbuf.at[s - 1, mixer_rows(h)],
+            dst_ref=mbuf.at[s - 1, mixer_rows(h)],
+            send_sem=e_s.at[e - 1, h, s - 1],
+            recv_sem=e_r.at[e - 1, h, s - 1],
+            device_id={"rep": lax.rem(rep + e, n_rep)},
+            device_id_type=MESH,
+        )
+
+    def columns(s):
         owner = lax.rem(fs - s + n_fs, n_fs)
         return pl.multiple_of(owner * depth, 128)
 
@@ -131,14 +149,19 @@
 
     for d in range(1, n_tp):
         ncopy(d).start()
-    for s in range(2, n_fs):
+    for s in range(1, n_fs):
         for h in range(2):
-            ring(0, h, s - 1).wait_recv()
-            ring(0, h, s).start()
-    ring(1, 0, 1).start()
-    ring(1, 1, 1).start()
-    for h in range(2):
-        ring(0, h, n_fs - 1).wait_recv()
+            ring(0, h, s).wait_recv()
+            if s < n_fs - 1:
+                ring(0, h, s + 1).start()
+                if s == n_fs - 2:
+                    ring(1, h, 1).start()
+            for e in range(1, n_rep):
+                across(h, s, e).start()
+    for s in range(1, n_fs):
+        for h in range(2):
+            for e in range(1, n_rep):
+                across(h, s, e).wait_recv()
     for d in range(1, n_tp):
         ncopy(d).wait_recv()
 
@@ -185,7 +208,11 @@
     at_t = lax.broadcasted_iota(jnp.int32, (span, span), 0)
     at_s = lax.broadcasted_iota(jnp.int32, (span, span), 1)
     mix_k = jnp.where(at_s <= at_t, mk_ref[group].astype(F32), 0.0).astype(BF16)
-    gain_part, shift_part, offset = lg_ref[tp], ls_ref[tp], mo_ref[group]
+    gain_part, shift_part = lg_ref[tp], ls_ref[tp]
+    offsets = mo_ref[...].astype(F32)
+    chosen = lax.broadcasted_iota(jnp.int32, offsets.shape, 0) == group
+    offset = jnp.sum(jnp.where(chosen, offsets, 0.0), axis=0, keepdims=True)
+    offset = jnp.broadcast_to(offset, (span, span)).T[:, 0:1]
 
     def mix(i, carry):
         rows = pl.ds(pl.multiple_of(i * tok, tok), tok)
@@ -265,7 +292,8 @@
         ring(1, h, n_fs - 1).wait_recv()
 
     gu = g_ref.shape[1]
-    hid = d_ref.shape[1]
+    hid = hbuf.shape[1]
+    packed = d_ref.shape[1] != hid
     chunk = 2 * tok
 
     def feed(i, carry):
@@ -289,13 +317,18 @@
         hbuf[rows, :] = hidden.astype(BF16)
         return carry
 
-    lax.fori_loop(0, n_g // 2, feed, 0)
-
-    def pcols(s, h):
-        return pl.ds(pl.multiple_of(columns(s) + h * part, part), part)
+    loops = n_g // 2
+    lax.fori_loop(0, loops // 2, feed, 0)
+    ring(2, 0, 1).wait_recv()
+    ring(2, 0, 2).start()
+    lax.fori_loop(loops // 2, loops, feed, 0)
 
     def down(s, h):
-        weights = block(2, s)[h * part : (h + 1) * part, :]
+        size = d_ref.shape[0] // 2
+        weights = block(2, s)[h * size : (h + 1) * size, :]
+        if packed:
+            turned = pltpu.roll(weights.astype(F32), half, 1).astype(BF16)
+            weights = jnp.concatenate([weights[:, :hid], turned[:, :hid]], axis=0)
 
         def one(i, carry):
             rows = pl.ds(pl.multiple_of(i * chunk, chunk), chunk)
@@ -318,9 +351,10 @@
     for s in range(n_fs):
         for h in range(2):
             if s > 0:
-                ring(2, h, s).wait_recv()
-                if s < n_fs - 1:
-                    ring(2, h, s + 1).start()
+                if (h, s) != (0, 1):
+                    ring(2, h, s).wait_recv()
+                    if s < n_fs - 1:
+                        ring(2, h, s + 1).start()
             down(s, h)
             for d in range(1, n_g):
                 pcopy(s, h, d).start()
@@ -343,6 +377,9 @@
         for h in range(2):
             for s in range(1, n_fs):
                 ring(p, h, s).wait_send()
+                if p == 0:
+                    for e in range(1, n_rep):
+                        across(h, s, e).wait_send()
     for d in range(1, n_tp):
         ncopy(d).wait_send()
         stcopy(d).wait_send()
@@ -390,18 +427,21 @@
     gate_half, up_half, down_half = (
         lax.dynamic_slice_in_dim(x, first, half, axis=1) for x in (ffn_gate, ffn_up, ffn_down)
     )
-    if (2 * half) % 128 == 0 and half % 128 != 0 and 2 * half >= hid and (2 * half) % 256 == 128:
+    part = depth // 2
+    if half % 128 == 64 and half > 64 and part % 256 == 0:
         gu = jnp.concatenate([gate_half, up_half], axis=1)
+        runs = [down_half[i * part // 2 : (i + 1) * part // 2] for i in range(4)]
+        down = jnp.concatenate(
+            [jnp.concatenate(runs[:2], axis=1), jnp.concatenate(runs[2:], axis=1)], axis=0
+        )
     else:
         gu = jnp.concatenate([pad_last(gate_half, hid), pad_last(up_half, hid)], axis=1)
-    down = pad_last(down_half, hid)
+        down = pad_last(down_half, hid)
     mixw = jnp.concatenate([pad_last(x, lwp) for x in (gate_proj, value_proj, out_proj)], axis=1)
     lgain = pad_last(layer_gain.astype(F32).reshape(n_tp, 1, lw), lwp)
     lshift = pad_last(layer_shift.astype(F32).reshape(n_tp, 1, lw), lwp)
-    offset = mix_offset.astype(F32)[:, :, None]
     n_g = n_rep * n_tp
     guw = gu.shape[1]
-    part = depth // 2
     sizes = (n_rep, n_fs, n_tp, width, lw, lwp, width // groups, half)
     vmem = pl.BlockSpec(memory_space=pltpu.VMEM)
     dma = pltpu.SemaphoreType.DMA
@@ -413,7 +453,7 @@
         scratch_shapes=[
             pltpu.VMEM((n_fs - 1, depth, 3 * lwp), BF16),
             pltpu.VMEM((n_fs - 1, depth, guw), BF16),
-            pltpu.VMEM((n_fs - 1, depth, hid), BF16),
+            pltpu.VMEM((n_fs - 1,) + down.shape, BF16),
             pltpu.VMEM((n_tp * tok, model), BF16),
             pltpu.VMEM((n_tp * tok, lwp), F32),
             pltpu.VMEM((n_tp * tok, lwp), F32),
@@ -427,6 +467,8 @@
             pltpu.VMEM((n_fs, 2, n_g - 1, tok, part), BF16),
             dma((3, 2, n_fs - 1)),
             dma((3, 2, n_fs - 1)),
+            dma((n_rep - 1, 2, n_fs - 1)),
+            dma((n_rep - 1, 2, n_fs - 1)),
             dma((n_tp - 1,)),
             dma((n_tp - 1,)),
             dma((n_tp - 1,)),
@@ -447,7 +489,7 @@
         lgain,
         lshift,
         mix_kernel,
-        offset,
+        mix_offset,
         ffn_gain.reshape(1, -1),
         mixw,
         gu,

time: 200 us -> 193 us (0.965)
  Pallas kernels: 189 us -> 178 us
  other arithmetic: 3.52 us -> 7.04 us
    pallas_call x1, Pallas kernels: 189 us -> 178 us  [per_device(): pl.pallas_call(functools.partial(kernel, sizes), out_shape=jax.ShapeDtype...]
where the time goes in v2:
time: 193 us; the launch traced here: 192 us
  Pallas kernels  178 us (92%)
  local copies, waits for them, and re-layouts  7.06 us (4%)
  other arithmetic  7.04 us (4%)
    pallas_call x1, Pallas kernels, per_device(): pl.pallas_call(functools.partial(kernel, sizes), out_shape=jax.ShapeDtype...  178 us

profile of v2, /device:TPU:1, one launch (start us, length us, event | category | flops | bytes accessed | tf_op | source)
XLA Modules:
  0.0 192.3 jit_solution(4106223786194094890)
XLA Ops:
  0.0 1.3 reshape.16.mg_ref
  1.3 1.3 reshape.22
  2.6 1.3 reshape.24
  3.8 1.3 reshape.21.fg_ref
  5.1 1.8 pad_maximum_fusion.3.m_ref
  6.9 2.2 %constant_dynamic-slice_fusion.1 = (bf16[512,704]{1,0:T(8,128)(2,1)S(1)}, bf16[512,704]{1,0:T(8,128)(2,1)S(1)}) fusion(bf16[512,1408]{1,0:T(8,128)(2,1)} %param.24, s32[]{:T(128)S(6)} %select_n.2, bf16[512,1408]{1,0:T(8,128)(2,1)} %param.23), kind=kLoop, calls=%fused_computation.6 | loop fusion | bytes 2883588 | tf_op jit(solution)/shard_map/dynamic_slice | solution.py:428
  9.1 0.0 copy-start
  9.2 1.6 pad_maximum_fusion.g_ref
  10.7 0.0 copy-done
  10.7 0.4 constant_dynamic-slice_fusion
  11.1 1.1 fusion.d_ref
  12.2 178.1 %shard_map.127 = bf16[128,2048]{1,0:T(8,128)(2,1)} custom-call(bf16[128,2048]{1,0:T(8,128)(2,1)} %tok_ref.1, bf16[1,2048]{1,0:T(2,128)(2,1)} %reshape.16.mg_ref, f32[4,1,128]{2,1,0:T(1,128)} %bitcast.2, f32[4,1,128]{2,1,0:T(1,128)} %bitcast.3, bf16[4,128,128]{2,1,0:T(8,128)(2,1)} %mk_ref.1, bf16[4,128]{1,0:T(4,128)(2,1)} %mo_ref.1, ...), custom_call_target="tpu_custom_call" | custom-call | tf_op jit(solution)/shard_map/pallas_call | solution.py:448
  190.4 1.9 copy.15
Async XLA Ops:
  9.1 1.6 copy-start
